TPU v7x, 32 devices: a whole 2x2x4 slice. The times are simulated.
32 devices in a mesh: sp: 8 (over z, x), tp: 4 (over y, core).
Axes of the slice: x: 2, y: 2, z: 4, core: 2. Of those that a mesh axis runs over, the one named last changes fastest.
Arguments:
- tokens: bfloat16 [3072, 2048], P(('sp', 'tp')), may hold values from -6 to 6
- norm_gain: float32 [2048], replicated, may hold values from 0.1 to 1.9
- w_recept: bfloat16 [2048, 1024], P(None, 'tp'), may hold values from -0.125 to 0.125
- w_key: bfloat16 [2048, 1024], P(None, 'tp'), may hold values from -0.125 to 0.125
- w_value: bfloat16 [2048, 1024], P(None, 'tp'), may hold values from -0.125 to 0.125
- w_decay: bfloat16 [2048, 1024], P(None, 'tp'), may hold values from -0.125 to 0.125
- w_rate: bfloat16 [2048, 1024], P(None, 'tp'), may hold values from -0.125 to 0.125
- w_gate: bfloat16 [2048, 1024], P(None, 'tp'), may hold values from -0.125 to 0.125
- shift_mix: float32 [3, 1024], P(None, 'tp'), may hold values from 0 to 1
- decay_base: float32 [1024], P('tp'), may hold values from -16 to -2
- rate_base: float32 [1024], P('tp'), may hold values from -10 to 1
- decay_drift: float32 [3072], P('sp'), may hold values from -2 to 2, as said below
- group_gain: float32 [1024], P('tp'), may hold values from 0.1 to 1.9
- initial_state: float32 [16, 64, 64], P('tp'), may hold values from -240 to 240
- w_out: bfloat16 [1024, 2048], replicated, may hold values from -0.1875 to 0.1875
Outputs:
- out: bfloat16 [3072, 2048], P(('sp', 'tp'))
Inputs may be any that keep to these rules, and one draw needn't show every extreme that they name: `decay_drift`: constant over aligned runs of 64 positions.
All inputs are finite; a program needn't handle non-finite values.
Results may differ from a plain program's by a relative error of at most 0.0083.
Values may be sent and summed in bfloat16 or wider, within the bound.
A program may use at most 128 MiB of HBM per device.

v0:
```python
import jax
import jax.numpy as jnp
from jax import lax
from jax.sharding import PartitionSpec as P

HEAD = 64
BLOCK = 64
norm_floor = 0.5
group_floor = 1.0
highest = lax.Precision.HIGHEST


def shifted_2(block, axis, distance):
    devices = range(lax.axis_size(axis))
    route = [(i - distance, i) for i in devices if i - distance in devices]
    return lax.ppermute(block, axis, route)


def carried_in(value, axis, join, neutral):
    count, mine = (lax.axis_size(axis), lax.axis_index(axis))
    pieces = jax.tree.map(lambda part: lax.all_gather(part, axis), value)
    running = jax.tree.map(
        lambda part, zero: jnp.full_like(part, 0) + jnp.asarray(zero, part.dtype), value, neutral
    )

    def turn(position, running):
        longer = join(running, jax.tree.map(lambda part: part[position], pieces))
        return jax.tree.map(lambda new, old: jnp.where(position < mine, new, old), longer, running)

    return lax.fori_loop(0, count - 1, turn, running)


def block_masks(width):
    places = lax.broadcasted_iota(jnp.int32, (width, width), 0)
    others = lax.broadcasted_iota(jnp.int32, (width, width), 1)
    return (others < places, others <= places)


def pair_dots(left, right):
    return jnp.einsum("bhtn,bhsn->bhts", left, right, precision=highest)


def chain_product(first, second):
    return jnp.einsum("hij,hjk->hik", first, second, precision=highest)


def prepare_blocks(streams):
    recept, decay, key, value, unit, rate = streams
    width = recept.shape[2]
    size = recept.shape[3]
    strict, inclusive = block_masks(width)
    logs = jnp.log(decay)
    running = jnp.cumsum(logs, axis=2)
    through = jnp.exp(running)
    until = jnp.exp(running - logs)
    alpha = -unit * until
    beta = unit * rate / through
    key_scaled = key / through
    recept_scaled = recept * through
    lower_ab = jnp.where(strict, pair_dots(alpha, beta), 0.0)
    lower_ak = jnp.where(strict, pair_dots(alpha, key_scaled), 0.0)
    system = jnp.eye(width, dtype=jnp.float32) - lower_ab
    targets = jnp.concatenate(
        [alpha, jnp.einsum("bhts,bhsr->bhtr", lower_ak, value, precision=highest)], axis=3
    )
    solved = jax.scipy.linalg.solve_triangular(system, targets, lower=True, unit_diagonal=True)
    solved_alpha = solved[..., :size]
    solved_value = solved[..., size:]
    final = through[:, :, -1:, :]
    beta_final = beta * final
    key_final = key_scaled * final
    transition = jnp.eye(size, dtype=jnp.float32) * final + jnp.einsum(
        "bhtm,bhtn->bhmn", solved_alpha, beta_final, precision=highest
    )
    added = jnp.einsum("bhtr,bhtn->bhrn", solved_value, beta_final, precision=highest) + jnp.einsum(
        "bhtr,bhtn->bhrn", value, key_final, precision=highest
    )
    upper_b = jnp.where(inclusive, pair_dots(recept_scaled, beta), 0.0)
    upper_k = jnp.where(inclusive, pair_dots(recept_scaled, key_scaled), 0.0)
    reads = recept_scaled + jnp.einsum("bhts,bhsn->bhtn", upper_b, solved_alpha, precision=highest)
    fixed_out = jnp.einsum(
        "bhts,bhsr->bhtr", upper_b, solved_value, precision=highest
    ) + jnp.einsum("bhts,bhsr->bhtr", upper_k, value, precision=highest)
    return (transition, added, reads, fixed_out)


def run_blocks(start, prepared, extra_rows):
    transition, added, reads, fixed_out = prepared
    added = jnp.concatenate(
        [added, jnp.zeros(added.shape[:2] + (extra_rows, added.shape[3]), jnp.float32)], axis=2
    )
    fixed_out = jnp.concatenate(
        [fixed_out, jnp.zeros(fixed_out.shape[:3] + (extra_rows,), jnp.float32)], axis=3
    )

    def block_step(state, inputs):
        trans_now, added_now, reads_now, fixed_now = inputs
        new_state = jnp.einsum("hrm,hmn->hrn", state, trans_now, precision=highest) + added_now
        readout = jnp.einsum("htn,hrn->htr", reads_now, state, precision=highest) + fixed_now
        return (new_state, readout)

    return lax.scan(block_step, start, (transition, added, reads, fixed_out))


def per_device(
    tokens,
    norm_gain,
    w_recept,
    w_key,
    w_value,
    w_decay,
    w_rate,
    w_gate,
    shift_mix,
    decay_base,
    rate_base,
    decay_drift,
    group_gain,
    initial_state,
    w_out,
):
    tok_float = tokens.astype(jnp.float32)
    normed = (
        tok_float
        * lax.rsqrt(jnp.mean(tok_float * tok_float, axis=-1, keepdims=True) + norm_floor)
        * norm_gain
    ).astype(jnp.bfloat16)
    weights = (w_recept, w_key, w_value, w_decay, w_rate, w_gate)
    piece = lax.all_gather(normed, "tp", axis=0, tiled=True)
    projected = jnp.stack(
        [
            jnp.dot(piece, weight, preferred_element_type=jnp.float32).astype(jnp.bfloat16)
            for weight in weights
        ],
        axis=0,
    )
    edge_rows = projected[0:3, -1:, :]
    earlier_rows = shifted_2(edge_rows, "sp", 1)
    current = projected[0:3].astype(jnp.float32)
    earlier = jnp.concatenate([earlier_rows.astype(jnp.float32), current[:, :-1]], axis=1)
    shifted = current + (earlier - current) * shift_mix[:, None, :]
    recept, key, value = (shifted[0], shifted[1], shifted[2])
    level = decay_base + projected[3].astype(jnp.float32) + decay_drift[:, None]
    decay = jnp.exp(-jnp.exp(-jax.nn.softplus(-level) - 0.5))
    rate = jax.nn.sigmoid(rate_base + projected[4].astype(jnp.float32))
    gate = jax.nn.sigmoid(projected[5].astype(jnp.float32))
    seq_rows, local_width = recept.shape
    local_heads = local_width // HEAD
    block_count = seq_rows // BLOCK

    def blocked(array):
        return array.reshape(block_count, BLOCK, local_heads, HEAD).transpose(0, 2, 1, 3)

    key_heads = key.reshape(seq_rows, local_heads, HEAD)
    unit = key_heads * lax.rsqrt(jnp.sum(key_heads * key_heads, axis=-1, keepdims=True) + 1.0)
    streams = (
        blocked(recept),
        blocked(decay),
        blocked(key),
        blocked(value),
        blocked(unit.reshape(seq_rows, local_width)),
        blocked(rate),
    )
    prepared = prepare_blocks(streams)
    identity = jnp.broadcast_to(jnp.eye(HEAD, dtype=jnp.float32), (local_heads, HEAD, HEAD))
    empty = jnp.zeros((local_heads, HEAD, HEAD), jnp.float32)
    start_state = jnp.concatenate([empty, identity], axis=1)

    def combine(earlier_pair, later_pair):
        first_map, first_add = earlier_pair
        second_map, second_add = later_pair
        return (
            chain_product(first_map, second_map),
            chain_product(first_add, second_map) + second_add,
        )

    stretch, readout = run_blocks(start_state, prepared, HEAD)
    prefix_map, prefix_add = carried_in(
        (stretch[:, HEAD:], stretch[:, :HEAD]), "sp", combine, (identity, empty)
    )
    carried = chain_product(initial_state, prefix_map) + prefix_add
    mixed = readout[..., :HEAD] + jnp.einsum(
        "bhtj,hvj->bhtv", readout[..., HEAD:], carried, precision=highest
    )
    center = mixed - jnp.mean(mixed, axis=-1, keepdims=True)
    spread = jnp.mean(center * center, axis=-1, keepdims=True)
    gains = group_gain.reshape(local_heads, HEAD)[None, :, None, :]
    scaled = center * lax.rsqrt(spread + group_floor) * gains
    flat = scaled.transpose(0, 2, 1, 3).reshape(seq_rows, local_width)
    gated = (flat * gate).astype(jnp.bfloat16)
    token_rows = lax.all_to_all(gated, "tp", split_axis=0, concat_axis=1, tiled=True)
    result = jnp.dot(token_rows, w_out, preferred_element_type=jnp.float32).astype(jnp.bfloat16)
    return result


def solution(mesh):
    return jax.shard_map(
        per_device,
        mesh=mesh,
        in_specs=(
            P(("sp", "tp"), None),
            P(),
            P(None, "tp"),
            P(None, "tp"),
            P(None, "tp"),
            P(None, "tp"),
            P(None, "tp"),
            P(None, "tp"),
            P(None, "tp"),
            P("tp"),
            P("tp"),
            P("sp"),
            P("tp"),
            P("tp", None, None),
            P(),
        ),
        out_specs=P(("sp", "tp"), None),
        check_vma=False,
    )
```

profile of v0, /device:TPU:0, one launch (start us, length us, event | category | flops | bytes accessed | tf_op | source)
XLA Modules:
  0.0 325.6 jit_solution(3846499401676920296)
XLA Ops:
  6.5 1.3 fusion.51
  7.8 1.9 fusion.53
  9.9 0.6 fusion.85
  11.2 0.8 concatenate.17
  11.9 0.6 iota_compare_fusion
  12.5 0.7 iota_compare_fusion.2
  13.2 19.1 %all-gather.4.cloned.1.call-done = bf16[384,2048]{1,0:T(8,128)(2,1)} async-done(((bf16[96,2048]{1,0:T(8,128)(2,1)}), bf16[384,2048]{1,0:T(8,128)(2,1)}) %all-gather.4.cloned.1.call-update) | async-done | bytes 1572880 | tf_op jit(solution)/shard_map/all_gather | solution.py:129
  32.3 2.1 fusion.48
  35.0 0.6 copy-done.27
  36.4 3.5 %collective-permute-start = (bf16[3,1,256]{2,1,0:T(2,128)(2,1)S(1)}, bf16[3,1,256]{2,1,0:T(2,128)(2,1)S(1)}, u32[]{:S(2)}, u32[]{:S(2)}) collective-permute-start(bf16[3,1,256]{2,1,0:T(2,128)(2,1)S(1)} %slice.58), channel_id=1, source_target_pairs={{0,4},{4,8},{8,12},{12,16},{16,20},{20,24},{24,28},{1,5},{5,9},{9,... | collective-permute-start | bytes 4616 | tf_op jit(solution)/shard_map/ppermute | solution.py:16
  40.0 1.6 fusion.81
  42.2 1.3 reshape.65
  43.4 1.3 log.10
  44.8 1.1 copy.125
  45.9 1.8 reduce_window_sum.11
  47.8 1.2 fusion.28
  48.9 1.1 fusion.89
  50.3 1.3 reshape_squeeze.10
  51.7 2.0 bitcast_divide_fusion.1
  53.8 2.4 convolution_select_fusion.2
  56.2 1.4 fusion.26
  57.6 118.6 %custom-call.4 = f32[6,4,1,64,64]{3,4,2,1,0:T(8,128)} custom-call(f32[6,4,1,64,64]{4,3,2,1,0:T(8,128)S(1)} %fusion.26), custom_call_target="InvertDiagBlocksLowerTriangular" | custom-call | tf_op jit(solution)/shard_map/jit(_solve_triangular)/vmap(vmap())/triangular_solve | solution.py:66
  176.2 1.3 reshape_squeeze.11
  177.6 0.9 copy-done.1
  178.5 2.2 fusion.61
  180.7 1.6 fusion.55
  182.3 2.3 convolution_add_fusion.4
  184.6 2.6 fusion.67
  187.2 2.2 reshape_squeeze.12
  189.4 2.7 convolution_select_fusion.1
  192.2 1.5 convolution_select_fusion
  193.7 1.9 convolution_add_fusion.2
  195.5 1.0 fusion.65
  196.9 1.7 convolution_add_fusion.3
  198.6 0.9 convolution_add_fusion.1
  199.7 0.7 copy-done.9
  200.5 18.9 %while.28 = (s32[]{:T(128)}, f32[4,128,64]{1,2,0:T(8,128)S(1)}, f32[6,4,64,128]{3,2,1,0:T(8,128)}, f32[6,4,64,64]{3,2,1,0:T(8,128)}, f32[6,4,128,64]{2,3,1,0:T(8...) while((s32[]{:T(128)}, f32[4,128,64]{1,2,0:T(8,128)S(1)}, ...), condition=%wide.region_4.5_spmd, body=%wide.region_3.4_spmd.sunk | while | flops 50397184 | bytes 1312861 | solution.py:102
  200.5 1.8 fusion.138
  202.3 1.3 fusion.137
  203.6 1.8 fusion.138
  205.5 1.3 fusion.137
  206.8 1.8 fusion.138
  208.6 1.3 fusion.137
  210.0 1.8 fusion.138
  211.8 1.3 fusion.137
  213.1 1.8 fusion.138
  214.9 1.3 fusion.137
  216.2 1.8 fusion.138
  218.1 1.3 fusion.137
  219.5 34.8 %all-gather.1 = f32[32,64,64]{2,1,0:T(8,128)} all-gather(f32[4,64,64]{2,1,0:T(8,128)S(1)} %get-tuple-element.240), channel_id=3, replica_groups=mesh['sp'=8,'tp'=4] {'sp'}, dimensions={0}, use_global_device_ids=true | all-gather | bytes 589824 | tf_op jit(solution)/shard_map/all_gather | solution.py:21
  254.4 32.6 %all-gather = f32[32,64,64]{2,1,0:T(8,128)S(1)} all-gather(f32[4,64,64]{2,1,0:T(8,128)S(1)} %get-tuple-element.241), channel_id=2, replica_groups=mesh['sp'=8,'tp'=4] {'sp'}, dimensions={0}, use_global_device_ids=true | all-gather | bytes 589824 | tf_op jit(solution)/shard_map/all_gather | solution.py:21
  287.0 13.2 %while.29 = (s32[]{:T(128)}, f32[4,64,64]{1,2,0:T(8,128)S(1)}, f32[4,64,64]{1,2,0:T(8,128)S(1)}, s32[]{:T(128)}, f32[8,4,64,64]{3,2,1,0:T(8,128)S(1)}, /*index=5*/f32[8,4,64,64]{3,2,1,0:T(8,128)}, s32[]{:T(128)}, s32[]{:T(128)}) while((s32[]{:T(128)}, f32[4,64,64]{1,2,0:T(8,128)S(1)}, f32[4,64,64]{1,2,0:T(8,128)S(1)}, s32[]{:T(128)}, ...), condition=%wide.region_6.7_spmd.clone, body=%wide.region_5.6_spmd.clone.sunk | while | flops 25247748 | bytes 1575032 | solution.py:30
  287.4 0.9 constant_dynamic-slice_fusion.2
  289.3 0.9 constant_dynamic-slice_fusion.2
  291.2 0.9 constant_dynamic-slice_fusion.2
  293.1 0.9 constant_dynamic-slice_fusion.2
  295.0 0.9 constant_dynamic-slice_fusion.2
  296.9 0.9 constant_dynamic-slice_fusion.2
  298.7 0.9 constant_dynamic-slice_fusion.2
  300.2 1.6 copy.66
  302.2 3.7 %fusion.91 = (f32[6,4,64]{2,0,1:T(8,128)S(1)}, f32[6,4,64,64]{2,3,0,1:T(8,128)S(1)}) fusion(f32[4,64,64,1]{1,2,3,0:T(8,128)S(1)} %fusion.50, f32[6,4,64,128]{2,3,0,1:T(8,128)S(1)} %copy.66, f32[6,4,64,128]{3,2,1,0:T(8,128)} %get-tuple-element.153), kind=kOutput, calls=%fused_computation.138 | convolution fusion | flops 75692544 | bytes 1644544 | tf_op jit(solution)/shard_map/bhtj,hvj->bhtv/dot_general | solution.py:182
  307.0 2.4 fusion.35
  309.5 7.7 %all_to_all.19 = bf16[4,96,256]{2,1,0:T(8,128)(2,1)S(1)} all-to-all(bf16[4,96,256]{2,1,0:T(8,128)(2,1)S(1)} %bitcast.170), channel_id=1, replica_groups=mesh['sp'=8,'tp'=4] {'tp'}, dimensions={0} | all-to-all | bytes 393216 | tf_op jit(solution)/shard_map/all_to_all | solution.py:191
  317.2 1.6 convolution_convert_fusion
  (138 shorter events, 11.7 us)
Async XLA Ops:
  6.5 25.7 %copy-start = (bf16[2048,256]{1,0:T(8,128)(2,1)S(1)}, bf16[2048,256]{1,0:T(8,128)(2,1)}, u32[]{:S(2)}) copy-start(bf16[2048,256]{1,0:T(8,128)(2,1)} %param.23) | copy-start | bytes 3145732
  6.5 3.3 %copy-start.24 = (f32[256]{0:T(256)S(1)}, f32[256]{0:T(256)}, u32[]{:S(2)}) copy-start(f32[256]{0:T(256)} %param.31) | copy-start | bytes 3076
  6.5 25.7 %all-gather.4.cloned.1.call-start = ((), (), s32[]{:S(2)}) async-start(), calls=%async_computation.1 | async-start | bytes 1966080 | tf_op jit(solution)/shard_map/all_gather | solution.py:129
  10.5 0.6 copy-start.15
  13.2 21.2 %copy-start.26 = (bf16[2048,256]{1,0:T(8,128)(2,1)S(1)}, bf16[2048,256]{1,0:T(8,128)(2,1)}, u32[]{:S(2)}) copy-start(bf16[2048,256]{1,0:T(8,128)(2,1)} %param.22) | copy-start | bytes 3145732
  32.3 2.1 copy-start.25
  34.4 1.2 copy-start.27
  36.2 5.4 %copy-start.13 = (bf16[1,384,256]{2,1,0:T(8,128)(2,1)}, bf16[1,384,256]{2,1,0:T(8,128)(2,1)S(1)}, u32[]{:S(2)}) copy-start(bf16[1,384,256]{2,1,0:T(8,128)(2,1)S(1)} %fusion.46) | copy-start | bytes 589828
  36.2 3.7 %copy-start.28 = (bf16[2048,256]{1,0:T(8,128)(2,1)S(1)}, bf16[2048,256]{1,0:T(8,128)(2,1)}, u32[]{:S(2)}) copy-start(bf16[2048,256]{1,0:T(8,128)(2,1)} %param.24) | copy-start | bytes 3145732
  36.2 3.7 %copy-start.30 = (f32[384]{0:T(512)S(1)}, f32[384]{0:T(512)}, u32[]{:S(2)}) copy-start(f32[384]{0:T(512)} %param.30) | copy-start | bytes 4612
  36.3 3.7 %copy-start.31 = (f32[256]{0:T(256)S(1)}, f32[256]{0:T(256)}, u32[]{:S(2)}) copy-start(f32[256]{0:T(256)} %param.28) | copy-start | bytes 3076
  36.4 5.2 %copy-start.29 = (bf16[2048,256]{1,0:T(8,128)(2,1)S(1)}, bf16[2048,256]{1,0:T(8,128)(2,1)}, u32[]{:S(2)}) copy-start(bf16[2048,256]{1,0:T(8,128)(2,1)} %param.25) | copy-start | bytes 3145732
  36.4 5.2 %copy-start.32 = (f32[256]{0:T(256)S(1)}, f32[256]{0:T(256)}, u32[]{:S(2)}) copy-start(f32[256]{0:T(256)} %param.29) | copy-start | bytes 3076
  36.4 11.3 %collective-permute-start = (bf16[3,1,256]{2,1,0:T(2,128)(2,1)S(1)}, bf16[3,1,256]{2,1,0:T(2,128)(2,1)S(1)}, u32[]{:S(2)}, u32[]{:S(2)}) collective-permute-start(bf16[3,1,256]{2,1,0:T(2,128)(2,1)S(1)} %slice.58), channel_id=1, source_target_pairs={{0,4},{4,8},{8,12},{12,16},{16,20},{20,24},{24,28},{1,5},{5,9},{9,... | collective-permute-start | bytes 4616 | tf_op jit(solution)/shard_map/ppermute | solution.py:16
  44.8 1.1 copy-start.5
  44.8 3.0 copy-start.23
  51.7 2.1 copy-start.3
  51.7 2.1 copy-start.21
  53.7 2.5 copy-start.6
  53.8 2.5 copy-start.16
  53.8 2.4 copy-start.18
  53.8 2.4 copy-start.22
  177.6 0.9 copy-start.1
  178.5 2.2 copy-start.7
  178.5 2.2 copy-start.14
  180.7 1.6 copy-start.17
  189.4 2.7 copy-start.4
  189.4 2.7 copy-start.8
  189.4 2.7 copy-start.20
  195.5 1.1 copy-start.2
  195.5 1.4 copy-start.12
  199.6 0.9 copy-start.9
  219.4 67.6 %copy-start.10 = (f32[4,64,64]{1,2,0:T(8,128)S(1)}, f32[4,64,64]{1,2,0:T(8,128)}, u32[]{:S(2)}) copy-start(f32[4,64,64]{1,2,0:T(8,128)} %custom-call.5) | copy-start | bytes 196612
  300.2 1.7 copy-start.19
  307.0 10.1 %copy-start.11 = (bf16[1024,2048]{1,0:T(8,128)(2,1)S(1)}, bf16[1024,2048]{1,0:T(8,128)(2,1)}, u32[]{:S(2)}) copy-start(bf16[1024,2048]{1,0:T(8,128)(2,1)} %param.33) | copy-start | bytes 12582916
Sparse Core Ops, SparseCore 0:
  9.9 22.3 all-gather.3
where the time goes:
time: 327 us; the launch traced here: 326 us
  other arithmetic  130 us (40%)
  blocking collectives  75.1 us (23%)
  matrix products  59.8 us (18%)
  local copies, waits for them, and re-layouts  23.2 us (7%)
  waiting for transfers between devices  19.1 us (6%)
  between operations  14 us (4%)
  starting transfers between devices  3.5 us (1%)
    another operation x2, other arithmetic, prepare_blocks(): jax.scipy.linalg.solve_triangular(system, targets, lower=True, unit_diago...  119 us
    all_gather x2, blocking collectives, carried_in(): pieces = jax.tree.map(lambda part: lax.all_gather(part, axis), value)  67.4 us
    all_gather x1, waiting for transfers between devices, per_device(): piece = lax.all_gather(normed, 'tp', axis=0, tiled=True)  19.1 us
    dot_general x6, matrix products, block_step(): jnp.einsum('htn,hrn->htr', reads_now, state, precision=highest) + fixed_now  10.9 us
    dot_general x4, matrix products, pair_dots(): return jnp.einsum('bhtn,bhsn->bhts', left, right, precision=highest)  8.01 us
    dot_general x6, matrix products, per_device(): jnp.dot(piece, weight, preferred_element_type=jnp.float32)  7.88 us
    dot_general x6, matrix products, block_step(): jnp.einsum('hrm,hmn->hrn', state, trans_now, precision=highest) + added_now  7.73 us
    all_to_all x1, blocking collectives, per_device(): lax.all_to_all(gated, 'tp', split_axis=0, concat_axis=1, tiled=True)  7.67 us
  transfers between devices with their start and end apart: 2, of which 1 were waited for; matrix products, arithmetic and copies ran while one was open for 3% of the time, Pallas kernels for 0%

commit v1 on v0

--- a/solution.py
+++ b/solution.py
@@ -126,7 +126,14 @@
         * norm_gain
     ).astype(jnp.bfloat16)
     weights = (w_recept, w_key, w_value, w_decay, w_rate, w_gate)
-    piece = lax.all_gather(normed, "tp", axis=0, tiled=True)
+    n_dev = lax.axis_size("tp")
+    forward = [(i_2, (i_2 + 1) % n_dev) for i_2 in range(n_dev)]
+    parts = [normed]
+    for stride in range(1, n_dev):
+        parts = [lax.ppermute(parts[0], "tp", forward), *parts]
+    whole = jnp.concatenate(parts, axis=0)
+    shift = (lax.axis_index("tp") + 1) * parts[-1].shape[0]
+    piece = jnp.roll(whole, shift, axis=0)
     projected = jnp.stack(
         [
             jnp.dot(piece, weight, preferred_element_type=jnp.float32).astype(jnp.bfloat16)

time: 327 us -> 314 us (0.960)
  between operations: 14 us -> 0.67 us
    all_gather x1 -> x0, waiting for transfers between devices: 19.1 us -> none  [per_device(): piece = lax.all_gather(normed, 'tp', axis=0, tiled=True)]
    ppermute x0 -> x3, waiting for transfers between devices: none -> 17.7 us  [per_device(): parts = [lax.ppermute(parts[0], 'tp', forward), *parts]]
  transfers between devices with their start and end apart: 2 -> 4, of which waited for: 1 -> 3; matrix products, arithmetic and copies ran while one was open for 3% -> 4% of each run, Pallas kernels for 0% -> 0%
where the time goes in v1:
time: 314 us; the launch traced here: 313 us
  other arithmetic  130 us (41%)
  blocking collectives  76.1 us (24%)
  matrix products  59.5 us (19%)
  local copies, waits for them, and re-layouts  23.2 us (7%)
  waiting for transfers between devices  17.7 us (6%)
  starting transfers between devices  4.86 us (2%)
    another operation x2, other arithmetic, prepare_blocks(): jax.scipy.linalg.solve_triangular(system, targets, lower=True, unit_diago...  119 us
    all_gather x2, blocking collectives, carried_in(): pieces = jax.tree.map(lambda part: lax.all_gather(part, axis), value)  68.5 us
    ppermute x3, waiting for transfers between devices, per_device(): parts = [lax.ppermute(parts[0], 'tp', forward), *parts]  17.7 us
    dot_general x6, matrix products, block_step(): jnp.einsum('htn,hrn->htr', reads_now, state, precision=highest) + fixed_now  11 us
    dot_general x4, matrix products, pair_dots(): return jnp.einsum('bhtn,bhsn->bhts', left, right, precision=highest)  7.94 us
    dot_general x6, matrix products, block_step(): jnp.einsum('hrm,hmn->hrn', state, trans_now, precision=highest) + added_now  7.73 us
    all_to_all x1, blocking collectives, per_device(): lax.all_to_all(gated, 'tp', split_axis=0, concat_axis=1, tiled=True)  7.67 us
    dynamic_slice x14, local copies, waits for them, and re-layouts, turn(): longer = join(running, jax.tree.map(lambda part: part[position], pieces))  7.11 us
  transfers between devices with their start and end apart: 4, of which 3 were waited for; matrix products, arithmetic and copies ran while one was open for 4% of the time, Pallas kernels for 0%

profile of v1, /device:TPU:0, one launch (start us, length us, event | category | flops | bytes accessed | tf_op | source)
XLA Modules:
  0.0 312.6 jit_solution(15672159589248534829)
XLA Ops:
  0.0 1.3 fusion.51
  1.3 1.2 fusion.53
  3.0 7.4 %collective-permute-done = bf16[96,2048]{1,0:T(8,128)(2,1)S(1)} collective-permute-done((bf16[96,2048]{1,0:T(8,128)(2,1)S(1)}, bf16[96,2048]{1,0:T(8,128)(2,1)S(1)}, u32[]{:S(2)}, u32[]{:S(2)}) %collective-permute-start) | collective-permute-done | bytes 393248 | tf_op jit(solution)/shard_map/ppermute | solution.py:133
  10.4 0.8 mul.139
  11.2 0.6 fusion.93
  12.4 0.8 concatenate.23
  13.2 4.4 %collective-permute-done.1 = bf16[96,2048]{1,0:T(8,128)(2,1)S(1)} collective-permute-done((bf16[96,2048]{1,0:T(8,128)(2,1)S(1)}, bf16[96,2048]{1,0:T(8,128)(2,1)S(1)}, u32[]{:S(2)}, u32[]{:S(2)}) %collective-permute-start.1) | collective-permute-done | bytes 393248 | tf_op jit(solution)/shard_map/ppermute | solution.py:133
  17.6 0.6 iota_compare_fusion
  18.2 0.7 iota_compare_fusion.2
  18.9 5.9 %collective-permute-done.2 = bf16[96,2048]{1,0:T(8,128)(2,1)S(1)} collective-permute-done((bf16[96,2048]{1,0:T(8,128)(2,1)S(1)}, bf16[96,2048]{1,0:T(8,128)(2,1)S(1)}, u32[]{:S(2)}, u32[]{:S(2)}) %collective-permute-start.2) | collective-permute-done | bytes 393248 | tf_op jit(solution)/shard_map/ppermute | solution.py:133
  28.3 4.3 %collective-permute-start.3 = (bf16[3,1,256]{2,1,0:T(2,128)(2,1)S(1)}, bf16[3,1,256]{2,1,0:T(2,128)(2,1)S(1)}, u32[]{:S(2)}, u32[]{:S(2)}) collective-permute-start(bf16[3,1,256]{2,1,0:T(2,128)(2,1)S(1)} %slice.58), channel_id=1, source_target_pairs={{0,4},{4,8},{8,12},{12,16},{16,20},{20,24},{24,28},{1,5},{5,9},{9,... | collective-permute-start | bytes 4616 | tf_op jit(solution)/shard_map/ppermute | solution.py:16
  32.7 1.6 fusion.87
  34.9 1.2 reshape.65
  36.1 1.3 log.10
  37.5 1.2 copy.125
  38.6 1.8 reduce_window_sum.11
  40.5 1.2 fusion.28
  41.7 1.1 fusion.103
  43.1 1.3 reshape_squeeze.10
  44.4 2.0 bitcast_divide_fusion.1
  46.5 2.4 convolution_select_fusion.2
  48.9 1.4 fusion.26
  50.3 118.6 %custom-call.4 = f32[6,4,1,64,64]{3,4,2,1,0:T(8,128)} custom-call(f32[6,4,1,64,64]{4,3,2,1,0:T(8,128)S(1)} %fusion.26), custom_call_target="InvertDiagBlocksLowerTriangular" | custom-call | tf_op jit(solution)/shard_map/jit(_solve_triangular)/vmap(vmap())/triangular_solve | solution.py:66
  168.9 1.3 reshape_squeeze.11
  170.3 0.9 copy-done.1
  171.1 2.1 fusion.61
  173.2 3.0 fusion.55
  176.2 2.3 convolution_add_fusion.4
  178.5 2.5 fusion.67
  181.0 2.3 reshape_squeeze.12
  183.3 2.7 convolution_select_fusion.1
  186.0 1.5 convolution_select_fusion
  187.5 1.9 convolution_add_fusion.2
  189.5 1.0 fusion.65
  190.4 1.7 convolution_add_fusion.3
  192.2 0.9 convolution_add_fusion.1
  193.3 18.9 %while.28 = (s32[]{:T(128)}, f32[4,128,64]{1,2,0:T(8,128)S(1)}, f32[6,4,64,128]{3,2,1,0:T(8,128)}, f32[6,4,64,64]{3,2,1,0:T(8,128)}, f32[6,4,128,64]{2,3,1,0:T(8...) while((s32[]{:T(128)}, f32[4,128,64]{1,2,0:T(8,128)S(1)}, ...), condition=%wide.region_4.5_spmd, body=%wide.region_3.4_spmd.sunk | while | flops 50397184 | bytes 1312861 | solution.py:102
  193.3 1.8 fusion.146
  195.1 1.3 fusion.145
  196.5 1.8 fusion.146
  198.3 1.3 fusion.145
  199.6 1.8 fusion.146
  201.5 1.3 fusion.145
  202.8 1.8 fusion.146
  204.6 1.3 fusion.145
  205.9 1.8 fusion.146
  207.8 1.3 fusion.145
  209.1 1.8 fusion.146
  210.9 1.3 fusion.145
  212.4 35.4 %all-gather.1 = f32[32,64,64]{2,1,0:T(8,128)} all-gather(f32[4,64,64]{2,1,0:T(8,128)S(1)} %get-tuple-element.240), channel_id=3, replica_groups=mesh['sp'=8,'tp'=4] {'sp'}, dimensions={0}, use_global_device_ids=true | all-gather | bytes 589824 | tf_op jit(solution)/shard_map/all_gather | solution.py:21
  247.8 33.1 %all-gather = f32[32,64,64]{2,1,0:T(8,128)S(1)} all-gather(f32[4,64,64]{2,1,0:T(8,128)S(1)} %get-tuple-element.241), channel_id=2, replica_groups=mesh['sp'=8,'tp'=4] {'sp'}, dimensions={0}, use_global_device_ids=true | all-gather | bytes 589824 | tf_op jit(solution)/shard_map/all_gather | solution.py:21
  280.9 13.2 %while.29 = (s32[]{:T(128)}, f32[4,64,64]{1,2,0:T(8,128)S(1)}, f32[4,64,64]{1,2,0:T(8,128)S(1)}, s32[]{:T(128)}, f32[8,4,64,64]{3,2,1,0:T(8,128)S(1)}, /*index=5*/f32[8,4,64,64]{3,2,1,0:T(8,128)}, s32[]{:T(128)}, s32[]{:T(128)}) while((s32[]{:T(128)}, f32[4,64,64]{1,2,0:T(8,128)S(1)}, f32[4,64,64]{1,2,0:T(8,128)S(1)}, s32[]{:T(128)}, ...), condition=%wide.region_6.7_spmd.clone, body=%wide.region_5.6_spmd.clone.sunk | while | flops 25247748 | bytes 1575032 | solution.py:30
  281.3 0.9 constant_dynamic-slice_fusion.2
  283.2 0.9 constant_dynamic-slice_fusion.2
  285.1 0.9 constant_dynamic-slice_fusion.2
  287.0 0.9 constant_dynamic-slice_fusion.2
  288.9 0.9 constant_dynamic-slice_fusion.2
  290.8 0.9 constant_dynamic-slice_fusion.2
  292.7 0.9 constant_dynamic-slice_fusion.2
  294.1 1.6 copy.66
  296.1 3.7 %fusion.105 = (f32[6,4,64]{2,0,1:T(8,128)S(1)}, f32[6,4,64,64]{2,3,0,1:T(8,128)S(1)}) fusion(f32[4,64,64,1]{1,2,3,0:T(8,128)S(1)} %fusion.50, f32[6,4,64,128]{2,3,0,1:T(8,128)S(1)} %copy.66, f32[6,4,64,128]{3,2,1,0:T(8,128)} %get-tuple-element.153), kind=kOutput, calls=%fused_computation.158 | convolution fusion | flops 75692544 | bytes 1644544 | tf_op jit(solution)/shard_map/bhtj,hvj->bhtv/dot_general | solution.py:189
  300.9 2.5 fusion.35
  303.3 7.7 %all_to_all.19 = bf16[4,96,256]{2,1,0:T(8,128)(2,1)S(1)} all-to-all(bf16[4,96,256]{2,1,0:T(8,128)(2,1)S(1)} %bitcast.164), channel_id=1, replica_groups=mesh['sp'=8,'tp'=4] {'tp'}, dimensions={0} | all-to-all | bytes 393216 | tf_op jit(solution)/shard_map/all_to_all | solution.py:198
  311.0 1.6 convolution_convert_fusion
  (147 shorter events, 13.7 us)
Async XLA Ops:
  0.0 25.4 %copy-start = (bf16[2048,256]{1,0:T(8,128)(2,1)S(1)}, bf16[2048,256]{1,0:T(8,128)(2,1)}, u32[]{:S(2)}) copy-start(bf16[2048,256]{1,0:T(8,128)(2,1)} %param.21) | copy-start | bytes 3145732
  0.0 24.9 %copy-start.9 = (bf16[96,2048]{1,0:T(8,128)(2,1)S(1)}, bf16[96,2048]{1,0:T(8,128)(2,1)}, u32[]{:S(2)}) copy-start(bf16[96,2048]{1,0:T(8,128)(2,1)} %param.19) | copy-start | bytes 1179652
  0.0 24.9 %copy-start.19 = (f32[2048]{0:T(1024)S(1)}, f32[2048]{0:T(1024)}, u32[]{:S(2)}) copy-start(f32[2048]{0:T(1024)} %param.20) | copy-start | bytes 24580
  2.5 8.0 %collective-permute-start = (bf16[96,2048]{1,0:T(8,128)(2,1)S(1)}, bf16[96,2048]{1,0:T(8,128)(2,1)S(1)}, u32[]{:S(2)}, u32[]{:S(2)}) collective-permute-start(bf16[96,2048]{1,0:T(8,128)(2,1)S(1)} %fusion.53), channel_id=1, source_target_pairs={{0,1},{1,2},{2,3},{3,0},{4,5},{5,6},{6,7},{7,4},{8,9},{9,10},{10,1... | collective-permute-start | bytes 1179656 | tf_op jit(solution)/shard_map/ppermute | solution.py:133
  10.4 7.2 %collective-permute-start.1 = (bf16[96,2048]{1,0:T(8,128)(2,1)S(1)}, bf16[96,2048]{1,0:T(8,128)(2,1)S(1)}, u32[]{:S(2)}, u32[]{:S(2)}) collective-permute-start(bf16[96,2048]{1,0:T(8,128)(2,1)S(1)} %collective-permute-done), channel_id=1, source_target_pairs={{0,1},{1,2},{2,3},{3,0},{4,5},{5,6},{6,7},{7,4},{8,9},{9,10},{10,1... | collective-permute-start | bytes 1179656 | tf_op jit(solution)/shard_map/ppermute | solution.py:133
  11.8 0.6 copy-start.14
  17.6 7.2 %collective-permute-start.2 = (bf16[96,2048]{1,0:T(8,128)(2,1)S(1)}, bf16[96,2048]{1,0:T(8,128)(2,1)S(1)}, u32[]{:S(2)}, u32[]{:S(2)}) collective-permute-start(bf16[96,2048]{1,0:T(8,128)(2,1)S(1)} %collective-permute-done.1), channel_id=1, source_target_pairs={{0,1},{1,2},{2,3},{3,0},{4,5},{5,6},{6,7},{7,4},{8,9},{9,10},{10,1... | collective-permute-start | bytes 1179656 | tf_op jit(solution)/shard_map/ppermute | solution.py:133
  25.1 1.3 copy-start.25
  25.4 8.9 %copy-start.20 = (bf16[768,2048]{1,0:T(8,128)(2,1)}, bf16[768,2048]{1,0:T(8,128)(2,1)S(1)}, u32[]{:S(2)}) copy-start(bf16[768,2048]{1,0:T(8,128)(2,1)S(1)} %constant_dynamic-update-slice_fusion) | copy-start | bytes 9437188
  25.4 2.1 copy-start.26
  27.5 5.1 %copy-start.27 = (bf16[2048,256]{1,0:T(8,128)(2,1)S(1)}, bf16[2048,256]{1,0:T(8,128)(2,1)}, u32[]{:S(2)}) copy-start(bf16[2048,256]{1,0:T(8,128)(2,1)} %param.24) | copy-start | bytes 3145732
  27.5 5.1 %copy-start.29 = (f32[384]{0:T(512)S(1)}, f32[384]{0:T(512)}, u32[]{:S(2)}) copy-start(f32[384]{0:T(512)} %param.30) | copy-start | bytes 4612
  27.5 5.1 %copy-start.30 = (f32[256]{0:T(256)S(1)}, f32[256]{0:T(256)}, u32[]{:S(2)}) copy-start(f32[256]{0:T(256)} %param.28) | copy-start | bytes 3076
  28.1 6.1 %copy-start.13 = (bf16[1,384,256]{2,1,0:T(8,128)(2,1)}, bf16[1,384,256]{2,1,0:T(8,128)(2,1)S(1)}, u32[]{:S(2)}) copy-start(bf16[1,384,256]{2,1,0:T(8,128)(2,1)S(1)} %fusion.48) | copy-start | bytes 589828
  28.1 6.1 %copy-start.28 = (bf16[2048,256]{1,0:T(8,128)(2,1)S(1)}, bf16[2048,256]{1,0:T(8,128)(2,1)}, u32[]{:S(2)}) copy-start(bf16[2048,256]{1,0:T(8,128)(2,1)} %param.25) | copy-start | bytes 3145732
  28.2 6.1 %copy-start.31 = (f32[256]{0:T(256)S(1)}, f32[256]{0:T(256)}, u32[]{:S(2)}) copy-start(f32[256]{0:T(256)} %param.29) | copy-start | bytes 3076
  28.3 12.2 %collective-permute-start.3 = (bf16[3,1,256]{2,1,0:T(2,128)(2,1)S(1)}, bf16[3,1,256]{2,1,0:T(2,128)(2,1)S(1)}, u32[]{:S(2)}, u32[]{:S(2)}) collective-permute-start(bf16[3,1,256]{2,1,0:T(2,128)(2,1)S(1)} %slice.58), channel_id=1, source_target_pairs={{0,4},{4,8},{8,12},{12,16},{16,20},{20,24},{24,28},{1,5},{5,9},{9,... | collective-permute-start | bytes 4616 | tf_op jit(solution)/shard_map/ppermute | solution.py:16
  34.9 5.6 %copy-start.24 = (f32[3,256]{1,0:T(4,128)S(1)}, f32[3,256]{1,0:T(4,128)}, u32[]{:S(2)}) copy-start(f32[3,256]{1,0:T(4,128)} %param.27) | copy-start | bytes 9220
  37.5 1.2 copy-start.5
  44.4 4.5 %copy-start.3 = (f32[6,64,4,64]{3,2,1,0:T(4,128)}, f32[6,64,4,64]{3,2,1,0:T(4,128)S(1)}, u32[]{:S(2)}) copy-start(f32[6,64,4,64]{3,2,1,0:T(4,128)S(1)} %reshape_squeeze.10) | copy-start | bytes 1179652
  44.4 2.1 copy-start.22
  46.4 2.4 copy-start.6
  46.5 2.4 copy-start.15
  46.5 2.4 copy-start.17
  46.5 2.4 copy-start.23
  170.3 0.9 copy-start.1
  171.1 5.1 %copy-start.16 = (f32[64,64]{1,0:T(8,128)S(1)}, f32[64,64]{1,0:T(8,128)}, u32[]{:S(2)}) copy-start(f32[64,64]{1,0:T(8,128)} %copy-done.14) | copy-start | bytes 49156
  183.3 2.7 copy-start.4
  183.3 2.7 copy-start.7
  183.3 2.7 copy-start.21
  187.5 2.9 copy-start.2
  187.5 2.9 copy-start.12
  192.2 1.1 copy-start.8
  212.2 68.6 %copy-start.10 = (f32[4,64,64]{1,2,0:T(8,128)S(1)}, f32[4,64,64]{1,2,0:T(8,128)}, u32[]{:S(2)}) copy-start(f32[4,64,64]{1,2,0:T(8,128)} %custom-call.5) | copy-start | bytes 196612
  280.9 14.8 %copy-start.18 = (f32[4,64,64]{2,1,0:T(8,128)S(1)}, f32[4,64,64]{2,1,0:T(8,128)}, u32[]{:S(2)}) copy-start(f32[4,64,64]{2,1,0:T(8,128)} %param.32) | copy-start | bytes 196612
  300.9 10.2 %copy-start.11 = (bf16[1024,2048]{1,0:T(8,128)(2,1)S(1)}, bf16[1024,2048]{1,0:T(8,128)(2,1)}, u32[]{:S(2)}) copy-start(bf16[1024,2048]{1,0:T(8,128)(2,1)} %param.33) | copy-start | bytes 12582916
